TPU v7x, 32 devices: a whole 2x2x4 slice. The times are simulated.
32 devices in a mesh: ep: 8 (over z, x), tp: 4 (over y, core).
Axes of the slice: x: 2, y: 2, z: 4, core: 2. Of those that a mesh axis runs over, the one named last changes fastest.
Arguments:
- stream: bfloat16 [128, 4096], P(None, 'ep'), may hold values from -6.5 to 6.5
- norm_gain: float32 [4096], P('ep'), may hold values from 0.1 to 1.9
- w_query: bfloat16 [4096, 2048], P('ep', 'tp'), may hold values from -0.09375 to 0.09375
- w_key: bfloat16 [4096, 1024], P('ep', 'tp'), may hold values from -0.09375 to 0.09375
- w_value: bfloat16 [4096, 1024], P('ep', 'tp'), may hold values from -0.09375 to 0.09375
- break_offset: float32 [16], P('tp'), may hold values from -10 to -2
- cache_keys: bfloat16 [128, 1024, 8, 128], P('ep', None, 'tp'), may hold values from -6 to 6
- cache_values: bfloat16 [128, 1024, 8, 128], P('ep', None, 'tp'), may hold values from -6 to 6
- lengths: int32 [128], P('ep'), may hold values from 128 to 1024
- w_output: bfloat16 [2048, 4096], P('tp', 'ep'), may hold values from -0.125 to 0.125
- head_gain: float32 [2048], P('tp'), may hold values from 0.1 to 1.9
- ffn_gain: float32 [4096], P('ep'), may hold values from 0.1 to 1.9
- route_experts: int32 [128, 2], replicated, may hold values from 0 to 7, all different within a row; in each aligned block of 128 rows (0 to 127, 128 to 255, ...) at most 64 rows name the same one
- route_weights: float32 [128, 2], replicated, may hold values from 0.1 to 1
- expert_gate: bfloat16 [8, 4096, 1024], P('ep', None, 'tp'), may hold values from -0.09375 to 0.09375
- expert_up: bfloat16 [8, 4096, 1024], P('ep', None, 'tp'), may hold values from -0.09375 to 0.09375
- expert_down: bfloat16 [8, 1024, 4096], P('ep', 'tp'), may hold values from -0.1875 to 0.1875
- dense_gate: bfloat16 [4096, 4096], P('ep', 'tp'), may hold values from -0.09375 to 0.09375
- dense_up: bfloat16 [4096, 4096], P('ep', 'tp'), may hold values from -0.09375 to 0.09375
- dense_down: bfloat16 [4096, 4096], P('tp', 'ep'), may hold values from -0.09375 to 0.09375
- mix_gain: float32 [4096], P('ep'), may hold values from 0.1 to 1.9
Outputs:
- mixed_out: bfloat16 [128, 4096], P(None, 'ep')
- key_rows: bfloat16 [128, 1024], P('ep', 'tp')
- value_rows: bfloat16 [128, 1024], P('ep', 'tp')
Inputs may be any that keep to these rules, and one draw needn't show every extreme that they name: `route_experts`: in the whole batch no expert is named by more than 64 pairs, a bound that some block reaches; the 2 experts of a token differ.
All inputs are finite; a program needn't handle non-finite values.
Results may differ from a plain program's by a relative error of at most 0.025.
Values may be sent and summed in bfloat16 or wider, within the bound.
A program may use at most 64 MiB of HBM per device.

v0:
```python
import jax
import jax.numpy as jnp
from jax import lax
from jax.sharding import PartitionSpec as P

EPSILON = 1e-06


def rms_scale(values, gain_vec, model_width):
    squares = lax.psum(jnp.sum(values * values, axis=1), "ep")
    return values * lax.rsqrt(squares / model_width + EPSILON)[:, None] * gain_vec[None, :]


def to_heads(normed, weights):
    return lax.psum_scatter(
        jnp.dot(normed, weights, preferred_element_type=jnp.float32).astype(jnp.bfloat16),
        "ep",
        scatter_dimension=0,
        tiled=True,
    ).astype(jnp.float32)


def from_heads(values, weights):
    partial_value = jnp.dot(
        lax.all_gather(values, "ep", axis=0, tiled=True),
        weights,
        preferred_element_type=jnp.float32,
    )
    return lax.psum(partial_value.astype(jnp.bfloat16), "tp")


def expert_terms(inputs, gate_w, up_w, down_w):
    gate_val = jnp.einsum("ecd,edf->ecf", inputs, gate_w, preferred_element_type=jnp.float32)
    up_val = jnp.einsum("ecd,edf->ecf", inputs, up_w, preferred_element_type=jnp.float32)
    hidden = (jax.nn.silu(gate_val) * up_val).astype(jnp.bfloat16)
    return jnp.einsum("ecf,efd->ecd", hidden, down_w, preferred_element_type=jnp.float32)


def slot_table(route_experts, experts, capacity):
    chosen = route_experts.reshape(-1)
    onehot = (chosen[:, None] == jnp.arange(experts, dtype=jnp.int32)[None, :]).astype(jnp.int32)
    earlier = jnp.cumsum(onehot, axis=0) - onehot
    rank_in = jnp.sum(earlier * onehot, axis=1)
    slot_ids = chosen * capacity + rank_in
    owners = jnp.arange(chosen.shape[0], dtype=jnp.int32) // route_experts.shape[1]
    filled = (
        jnp.full((experts * capacity,), route_experts.shape[0], jnp.int32).at[slot_ids].set(owners)
    )
    return (slot_ids, filled)


def per_device(
    stream,
    norm_gain,
    w_query,
    w_key,
    w_value,
    break_offset,
    cache_keys,
    cache_values,
    lengths,
    w_output,
    head_gain,
    ffn_gain,
    route_experts,
    route_weights,
    expert_gate,
    expert_up,
    expert_down,
    dense_gate,
    dense_up,
    dense_down,
    mix_gain,
):
    model_width = stream.shape[1] * lax.axis_size("ep")
    block_width = stream.shape[1]
    seq_count = lengths.shape[0]
    kv_local = cache_keys.shape[2]
    head_dim = cache_keys.shape[3]
    heads_local = break_offset.shape[0]
    group_size = heads_local // kv_local
    cache_len = cache_keys.shape[1]
    streamf = stream.astype(jnp.float32)
    normed = rms_scale(streamf, norm_gain, model_width).astype(jnp.bfloat16)
    projected = to_heads(normed, jnp.concatenate([w_query, w_key, w_value], axis=1))
    q_width = w_query.shape[1]
    k_width = w_key.shape[1]
    queries = (
        projected[:, :q_width]
        .astype(jnp.bfloat16)
        .reshape(seq_count, kv_local, group_size, head_dim)
    )
    key_rows = projected[:, q_width : q_width + k_width].astype(jnp.bfloat16)
    value_rows = projected[:, q_width + k_width :].astype(jnp.bfloat16)
    scores = jnp.einsum("skgd,slkd->skgl", queries, cache_keys, preferred_element_type=jnp.float32)
    scores = (
        scores * head_dim ** (-0.5) + break_offset.reshape(kv_local, group_size)[None, :, :, None]
    )
    in_cache = (jnp.arange(cache_len, dtype=jnp.int32)[None, :] < lengths[:, None])[
        :, None, None, :
    ]
    failed = jnp.where(in_cache, jax.nn.log_sigmoid(-scores), 0.0)
    later_sum = lax.cumsum(failed, axis=3, reverse=True) - failed
    weights = jnp.where(in_cache, jnp.exp(jax.nn.log_sigmoid(scores) + later_sum), 0.0).astype(
        jnp.bfloat16
    )
    attended = jnp.einsum(
        "skgl,slkd->skgd", weights, cache_values, preferred_element_type=jnp.float32
    )
    gains = head_gain.reshape(kv_local, group_size, head_dim)[None]
    normalized = (
        attended * lax.rsqrt(jnp.mean(attended * attended, axis=3, keepdims=True) + EPSILON) * gains
    )
    head_out = normalized.astype(jnp.bfloat16).reshape(seq_count, heads_local * head_dim)
    attn_out = from_heads(head_out, w_output)
    residual = streamf + attn_out.astype(jnp.float32)
    normed_ffn = rms_scale(residual, ffn_gain, model_width).astype(jnp.bfloat16)
    dense_width = dense_gate.shape[1]
    gate_up = to_heads(normed_ffn, jnp.concatenate([dense_gate, dense_up], axis=1))
    dense_hidden = (jax.nn.silu(gate_up[:, :dense_width]) * gate_up[:, dense_width:]).astype(
        jnp.bfloat16
    )
    dense_out = from_heads(dense_hidden, dense_down)
    experts = expert_gate.shape[0] * lax.axis_size("ep")
    capacity = 2 * seq_count * route_experts.shape[1] // expert_gate.shape[0]
    slot_ids, filled = slot_table(route_experts, experts, capacity)
    padded = jnp.concatenate([normed_ffn, jnp.zeros((1, block_width), jnp.bfloat16)], axis=0)
    outgoing = padded[filled].reshape(experts, capacity, block_width)
    slot_share = capacity // lax.axis_size("tp")
    own_slots = lax.dynamic_slice_in_dim(outgoing, lax.axis_index("tp") * slot_share, slot_share, 1)
    arrived = lax.all_to_all(own_slots, "ep", split_axis=0, concat_axis=2, tiled=True)
    gathered = lax.all_gather(arrived, "tp", axis=1, tiled=True)
    partial_value = expert_terms(gathered, expert_gate, expert_up, expert_down)
    summed = lax.psum_scatter(
        partial_value.astype(jnp.bfloat16), "tp", scatter_dimension=1, tiled=True
    )
    came_back = lax.all_to_all(summed, "ep", split_axis=2, concat_axis=0, tiled=True)
    returned = lax.all_gather(came_back, "tp", axis=1, tiled=True)
    picked = returned.reshape(experts * capacity, block_width)[slot_ids]
    picked = picked.reshape(route_experts.shape[0], route_experts.shape[1], block_width).astype(
        jnp.float32
    )
    shares = route_weights / jnp.sum(route_weights, axis=1, keepdims=True)
    moe_out = jnp.sum(picked * shares[:, :, None], axis=1)
    mixed_out = (residual + moe_out + mix_gain[None, :] * dense_out.astype(jnp.float32)).astype(
        jnp.bfloat16
    )
    return (mixed_out, key_rows, value_rows)


def solution(mesh):
    in_specs = (
        P(None, "ep"),
        P("ep"),
        P("ep", "tp"),
        P("ep", "tp"),
        P("ep", "tp"),
        P("tp"),
        P("ep", None, "tp", None),
        P("ep", None, "tp", None),
        P("ep"),
        P("tp", "ep"),
        P("tp"),
        P("ep"),
        P(),
        P(),
        P("ep", None, "tp"),
        P("ep", None, "tp"),
        P("ep", "tp", None),
        P("ep", "tp"),
        P("ep", "tp"),
        P("tp", "ep"),
        P("ep"),
    )
    out_specs = (P(None, "ep"), P("ep", "tp"), P("ep", "tp"))
    return jax.shard_map(
        per_device, mesh=mesh, in_specs=in_specs, out_specs=out_specs, check_vma=False
    )
```

profile of v0, /device:TPU:0, one launch (start us, length us, event | category | flops | bytes accessed | tf_op | source)
XLA Modules:
  0.0 456.8 jit_solution(16024287437481387308)
XLA Ops:
  7.3 1.1 fusion.35
  8.4 23.1 %psum.28 = f32[128]{0:T(128)S(1)} all-reduce(f32[128]{0:T(128)S(1)} %fusion.35), channel_id=1, replica_groups=mesh['ep'=8,'tp'=4] {'ep'}, use_global_device_ids=true, to_apply=%region_1.0 | all-reduce | flops 128 | bytes 1024 | tf_op jit(solution)/shard_map/psum | solution.py:10
  31.5 2.3 convolution_convert_fusion.2
  34.5 0.6 reduce-window.16
  35.0 0.2 slice_reduce_fusion
  35.7 1.4 scatter_custom_fusion
  37.2 56.6 %reduce-scatter.4.cloned.1.call-done = bf16[16,1024]{1,0:T(8,128)(2,1)} async-done(((bf16[128,1024]{1,0:T(8,128)(2,1)}), bf16[16,1024]{1,0:T(8,128)(2,1)}) %reduce-scatter.4.cloned.1.call-update) | async-done | bytes 32784 | tf_op jit(solution)/shard_map/reduce_scatter | solution.py:15
  93.8 0.7 slice.43
  94.5 5.7 %fusion.42 = (f32[16,2,2,1024]{3,2,1,0:T(2,128)S(1)}, f32[16,2,2,1024]{3,2,1,0:T(2,128)S(1)}) fusion(pred[16,1024]{1,0:T(8,128)(4,1)S(1)} %iota_compare_fusion, f32[2,2]{1,0:T(2,128)S(1)} %add.104, bf16[16,2,2,128]{3,2,1,0:T(2,128)(2,1)S(1)} %reshape.137, bf16[16,1024,2,128]{3,2,1,0:T(2,128)(2,1)} %param.27), kind=kOutput, calls=%fused_computation.45 | convolution fusion | flops 17432576 | bytes 8945680 | tf_op jit(solution)/shard_map/skgd,slkd->skgl/dot_general | solution.py:95
  100.2 0.2 reshape.138
  100.4 79.2 %reduce-window.14 = f32[16,2,2,8,128]{4,3,2,1,0:T(8,128)S(1)} reduce-window(f32[16,2,2,8,128]{4,3,2,1,0:T(8,128)S(1)} %reshape.138, f32[]{:T(128)} %constant.27.clone.1), window={size=1x1x1x1x128 pad=0_0x0_0x0_0x0_0x0_127}, to_apply=%region_3.4 | reduce-window | flops 8323072 | bytes 524292 | tf_op jit(solution)/shard_map/reduce-window
  179.7 0.3 copy.78
  180.4 5.9 %multiply_reduce_fusion.2 = (f32[16,2,2]{2,1,0:T(2,128)S(1)}, f32[16,2,2,128]{3,2,1,0:T(2,128)S(1)}) fusion(bf16[16,1024,2,128]{3,2,1,0:T(2,128)(2,1)} %param.28, pred[16,1024]{1,0:T(8,128)(4,1)S(1)} %iota_compare_fusion, f32[16,2,2,1024]{3,2,1,0:T(2,128)S(1)} %reduce_window_sum.30, f32[16,2,2,1024]{3,2,1,0:T(2,128)S(1)} %get-tuple-element.6), kind=kOutput, calls=%fused_computation.65 | convolution fusion | flops 18104256 | bytes 8962304 | tf_op jit(solution)/shard_map/skgl,slkd->skgd/dot_general | solution.py:107
  186.7 30.6 %all_gather.12 = bf16[128,512]{1,0:T(8,128)(2,1)S(1)} all-gather(bf16[16,512]{1,0:T(8,128)(2,1)S(1)} %reshape.140), channel_id=1, replica_groups=mesh['ep'=8,'tp'=4] {'ep'}, dimensions={0}, use_global_device_ids=true | all-gather | bytes 147456 | tf_op jit(solution)/shard_map/all_gather | solution.py:25
  217.2 0.9 convolution_convert_fusion.3
  218.2 31.0 %all-reduce.4.cloned.1.call-done = bf16[128,512]{1,0:T(8,128)(2,1)} async-done(((bf16[128,512]{1,0:T(8,128)(2,1)}), bf16[128,512]{1,0:T(8,128)(2,1)}) %all-reduce.4.cloned.1.call-update) | async-done | bytes 131088 | tf_op jit(solution)/shard_map/psum | solution.py:29
  249.1 1.0 multiply_reduce_fusion.1
  250.1 21.3 %psum.30 = f32[128]{0:T(128)S(1)} all-reduce(f32[128]{0:T(128)S(1)} %multiply_reduce_fusion.1), channel_id=1, replica_groups=mesh['ep'=8,'tp'=4] {'ep'}, use_global_device_ids=true, to_apply=%region_8.9 | all-reduce | flops 128 | bytes 1024 | tf_op jit(solution)/shard_map/psum | solution.py:10
  271.5 1.0 multiply_convert_fusion
  272.5 2.0 gather_fusion
  274.5 0.7 constant_dynamic-slice_fusion
  275.2 3.4 all-to-all-start
  278.6 2.8 convolution_convert_fusion.1
  281.5 4.4 all-to-all-done
  285.9 6.7 %all_gather.13 = bf16[1,64,4096]{2,1,0:T(8,128)(2,1)S(1)} all-gather(bf16[1,16,4096]{2,1,0:T(8,128)(2,1)S(1)} %bitcast.68), channel_id=1, replica_groups=mesh['ep'=8,'tp'=4] {'tp'}, dimensions={1}, use_global_device_ids=true | all-gather | bytes 655360 | tf_op jit(solution)/shard_map/all_gather | solution.py:132
  292.5 2.1 fusion.11
  294.6 3.8 fusion.4
  298.5 0.7 copy.91
  299.3 0.6 fusion.64
  299.9 46.4 %reduce-scatter.8.cloned.1.call-done = bf16[16,2048]{1,0:T(8,128)(2,1)} async-done(((bf16[128,2048]{1,0:T(8,128)(2,1)}), bf16[16,2048]{1,0:T(8,128)(2,1)}) %reduce-scatter.8.cloned.1.call-update) | async-done | bytes 65552 | tf_op jit(solution)/shard_map/reduce_scatter | solution.py:15
  346.2 0.8 convert_element_type.85
  347.1 30.8 %all_gather.15 = bf16[128,1024]{1,0:T(8,128)(2,1)S(1)} all-gather(bf16[16,1024]{1,0:T(8,128)(2,1)S(1)} %fusion.47), channel_id=1, replica_groups=mesh['ep'=8,'tp'=4] {'ep'}, dimensions={0}, use_global_device_ids=true | all-gather | bytes 294912 | tf_op jit(solution)/shard_map/all_gather | solution.py:25
  378.0 4.9 %copy.87 = bf16[1,16,4096]{1,0,2:T(2,128)(2,1)} copy(bf16[1,16,4096]{2,1,0:T(8,128)(2,1)} %reduce-scatter.6.cloned.1.call-done) | data formatting | bytes 262144 | tf_op jit(solution)/shard_map/reduce_scatter | solution.py:134
  382.9 0.5 broadcast.126
  383.4 23.4 %reduce.2 = bf16[4096,16]{1,0:T(8,128)(2,1)S(1)} reduce(bf16[4096,1,16]{2,1,0:T(2,128)(2,1)} %bitcast.64, bf16[]{:T(256)} %broadcast.126), dimensions={1}, to_apply=%bitcast.53.reduce_sub_computation | reduce | bytes 262146
  406.8 1.7 reshape.179
  408.5 3.4 all-to-all-start.1
  412.0 2.2 convolution_convert_fusion.4
  414.2 5.1 %all-to-all-done.1 = bf16[8,2,4096]{2,1,0:T(2,128)(2,1)S(1)} async-done(((bf16[8,2,4096]{2,1,0:T(2,128)(2,1)}), bf16[8,2,4096]{2,1,0:T(2,128)(2,1)S(1)}, u32[]{:S(2)}, u32[]{:S(2)}) %all-to-all-start.1) | async-done | bytes 131104 | tf_op jit(solution)/shard_map/all_to_all | solution.py:137
  419.3 3.9 reshape.180
  423.2 4.4 copy.88
  427.7 7.2 %all-gather = bf16[8,1,64,512]{3,0,1,2:T(8,128)(2,1)S(1)} all-gather(bf16[8,1,16,512]{3,0,1,2:T(8,128)(2,1)S(1)} %bitcast_bitcast_fusion), channel_id=2, replica_groups=mesh['ep'=8,'tp'=4] {'tp'}, dimensions={2}, use_global_device_ids=true | all-gather | bytes 655360 | tf_op jit(solution)/shard_map/all_gather | solution.py:138
  434.8 0.2 copy.90
  435.0 1.2 gather_fusion.1
  436.2 0.3 reshape.148
  436.5 0.7 multiply_reduce_fusion
  437.2 11.4 %all-reduce.6.cloned.1.call-done = bf16[128,512]{1,0:T(8,128)(2,1)} async-done(((bf16[128,512]{1,0:T(8,128)(2,1)}), bf16[128,512]{1,0:T(8,128)(2,1)}) %all-reduce.6.cloned.1.call-update) | async-done | bytes 131088 | tf_op jit(solution)/shard_map/psum | solution.py:29
  448.6 1.6 add_convert_fusion
  (74 shorter events, 2.2 us)
Async XLA Ops:
  7.2 287.4 %copy-start = (bf16[1,256,4096]{2,1,0:T(8,128)(2,1)S(1)}, bf16[1,256,4096]{2,1,0:T(8,128)(2,1)}, u32[]{:S(2)}) copy-start(bf16[1,256,4096]{2,1,0:T(8,128)(2,1)} %param.37) | copy-start | bytes 6291460
  7.2 26.8 %copy-start.6 = (s32[128,2]{0,1:T(2,128)S(1)}, s32[128,2]{0,1:T(2,128)}, u32[]{:S(2)}) copy-start(s32[128,2]{0,1:T(2,128)} %param.33) | copy-start | bytes 3076
  7.2 27.2 %copy-start.12 = (f32[4]{0:T(128)S(1)}, f32[4]{0:T(128)}, u32[]{:S(2)}) copy-start(f32[4]{0:T(128)} %param.26) | copy-start | bytes 52
  7.2 29.9 %copy-start.11 = (s32[16]{0:T(128)S(1)}, s32[16]{0:T(128)}, u32[]{:S(2)}) copy-start(s32[16]{0:T(128)} %param.29) | copy-start | bytes 196
  7.2 86.6 %reduce-scatter.4.cloned.1.call-start = ((), (), s32[]{:S(2)}) async-start(), calls=%async_computation.5 | async-start | bytes 294912 | tf_op jit(solution)/shard_map/reduce_scatter | solution.py:15
  33.9 215.2 %all-reduce.4.cloned.1.call-start = ((), (), s32[]{:S(2)}) async-start(), calls=%async_computation.6 | async-start | bytes 262144 | tf_op jit(solution)/shard_map/psum | solution.py:29
  180.4 6.1 %copy-start.10 = (f32[512]{0:T(512)S(1)}, f32[512]{0:T(512)}, u32[]{:S(2)}) copy-start(f32[512]{0:T(512)} %param.31) | copy-start | bytes 6148
  180.4 36.8 %copy-start.3 = (bf16[512,512]{1,0:T(8,128)(2,1)S(1)}, bf16[512,512]{1,0:T(8,128)(2,1)}, u32[]{:S(2)}) copy-start(bf16[512,512]{1,0:T(8,128)(2,1)} %param.30) | copy-start | bytes 1572868
  180.4 68.7 %copy-start.1 = (bf16[128,512]{1,0:T(8,128)(2,1)S(1)}, bf16[128,512]{1,0:T(8,128)(2,1)}, u32[]{:S(2)}) copy-start(bf16[128,512]{1,0:T(8,128)(2,1)} %param.21) | copy-start | bytes 393220
  180.4 91.1 %copy-start.8 = (f32[512]{0:T(512)S(1)}, f32[512]{0:T(512)}, u32[]{:S(2)}) copy-start(f32[512]{0:T(512)} %param.32) | copy-start | bytes 6148
  275.2 10.7 %all-to-all-start = ((bf16[8,16,512]{2,1,0:T(8,128)(2,1)}), bf16[8,16,512]{2,1,0:T(8,128)(2,1)S(1)}, u32[]{:S(2)}, u32[]{:S(2)}) async-start(bf16[8,16,512]{2,1,0:T(8,128)(2,1)} %constant_dynamic-slice_fusion), calls=%async_computation.1 | async-start | bytes 262144 | tf_op jit(solution)/shard_map/all_to_all | solution.py:131
  278.6 67.7 %reduce-scatter.8.cloned.1.call-start = ((), (), s32[]{:S(2)}) async-start(), calls=%async_computation.8 | async-start | bytes 589824 | tf_op jit(solution)/shard_map/reduce_scatter | solution.py:15
  281.4 96.5 %reduce-scatter.6.cloned.1.call-start = ((), (), s32[]{:S(2)}) async-start(), calls=%async_computation.7 | async-start | bytes 655360 | tf_op jit(solution)/shard_map/reduce_scatter | solution.py:134
  294.6 3.9 copy-start.7
  294.6 4.6 %copy-start.5 = (bf16[16,1024]{1,0:T(8,128)(2,1)S(1)}, bf16[16,1024]{1,0:T(8,128)(2,1)}, u32[]{:S(2)}) copy-start(bf16[16,1024]{1,0:T(8,128)(2,1)} %reduce-scatter.4.cloned.1.call-done) | copy-start | bytes 98308
  408.5 10.7 %all-to-all-start.1 = ((bf16[8,2,4096]{2,1,0:T(2,128)(2,1)}), bf16[8,2,4096]{2,1,0:T(2,128)(2,1)S(1)}, u32[]{:S(2)}, u32[]{:S(2)}) async-start(bf16[8,2,4096]{2,1,0:T(2,128)(2,1)} %reshape.179), calls=%async_computation.3 | async-start | bytes 262144 | tf_op jit(solution)/shard_map/all_to_all | solution.py:137
  411.9 36.7 %all-reduce.6.cloned.1.call-start = ((), (), s32[]{:S(2)}) async-start(), calls=%async_computation.9 | async-start | bytes 262144 | tf_op jit(solution)/shard_map/psum | solution.py:29
  434.8 1.7 copy-start.4
  435.0 13.6 %copy-start.2 = (bf16[128,512]{1,0:T(8,128)(2,1)S(1)}, bf16[128,512]{1,0:T(8,128)(2,1)}, u32[]{:S(2)}) copy-start(bf16[128,512]{1,0:T(8,128)(2,1)} %all-reduce.4.cloned.1.call-done) | copy-start | bytes 393220
  435.0 13.6 %copy-start.9 = (f32[512]{0:T(512)S(1)}, f32[512]{0:T(512)}, u32[]{:S(2)}) copy-start(f32[512]{0:T(512)} %param.41) | copy-start | bytes 6148
Sparse Core Ops, SparseCore 0:
  34.0 59.7 reduce-scatter.3
  218.3 30.8 all-reduce.3
  282.7 63.4 reduce-scatter.7
  348.6 20.6 reduce-scatter.5
  415.3 33.2 all-reduce.5
where the time goes:
time: 458 us; the launch traced here: 457 us
  waiting for transfers between devices  155 us (34%)
  blocking collectives  120 us (26%)
  other arithmetic  110 us (24%)
  matrix products  25.7 us (6%)
  local copies, waits for them, and re-layouts  25.2 us (6%)
  between operations  14.2 us (3%)
  starting transfers between devices  6.96 us (2%)
    reduce_scatter x2, waiting for transfers between devices, to_heads(): lax.psum_scatter(jnp.dot(normed, weights, preferred_element_type=jnp.floa...  103 us
    another operation x4, other arithmetic  79.9 us
    all_gather x2, blocking collectives, from_heads(): lax.all_gather(values, 'ep', axis=0, tiled=True)  61.4 us
    psum x2, blocking collectives, rms_scale(): squares = lax.psum(jnp.sum(values * values, axis=1), 'ep')  44.5 us
    psum x2, waiting for transfers between devices, from_heads(): return lax.psum(partial_value.astype(jnp.bfloat16), 'tp')  42.3 us
    unnamed x1, other arithmetic  23.4 us
  transfers between devices with their start and end apart: 7, of which 6 were waited for; matrix products, arithmetic and copies ran while one was open for 6% of the time, Pallas kernels for 0%

commit v1 on v0

v1 whole, which is shorter than its diff:
```python
import functools

import jax
import jax.numpy as jnp
from jax import lax
from jax.experimental import pallas as pl
from jax.experimental.pallas import tpu as pltpu
from jax.sharding import PartitionSpec as P

EPSILON = 1e-06
MESH = pl.DeviceIdType.MESH
F32 = jnp.float32
BF16 = jnp.bfloat16
NT = (((1,), (1,)), ((), ()))


def row_sums(squares):
    ones = jnp.ones((8, squares.shape[1]), BF16)
    high = squares.astype(BF16)
    low = (squares - high.astype(F32)).astype(BF16)
    return lax.dot_general(ones, high, NT, preferred_element_type=F32) + lax.dot_general(
        ones, low, NT, preferred_element_type=F32
    )


def own_column(sums, first, rows):
    width = sums.shape[1]
    lane = lax.broadcasted_iota(jnp.int32, (rows, width), 1)
    row = lax.broadcasted_iota(jnp.int32, (rows, width), 0)
    return jnp.sum(jnp.where(lane == row + first, sums[0:1, :], 0.0), axis=1, keepdims=True)


def greet(axes):
    barrier = pltpu.get_barrier_semaphore()
    total = 0
    for axis, count in axes:
        me = lax.axis_index(axis)
        for k in range(1, count):
            pl.semaphore_signal(
                barrier, inc=1, device_id={axis: lax.rem(me + k, count)}, device_id_type=MESH
            )
            total += 1
    pl.semaphore_wait(barrier, total)


def send(axis, count, k, src, dst, send_sem, recv_sem):
    peer = lax.rem(lax.axis_index(axis) + k, count)
    copy = pltpu.make_async_remote_copy(
        src_ref=src,
        dst_ref=dst,
        send_sem=send_sem.at[k - 1],
        recv_sem=recv_sem.at[k - 1],
        device_id={axis: peer},
        device_id_type=MESH,
    )
    copy.start()
    return copy


def project_kernel(
    n, width, x_ref, g_ref, wq_ref, wk_ref, wv_ref, q_ref, k_ref, v_ref,
    part, sums, got, got_sums, s_send, s_recv, p_send, p_recv,
):
    me = lax.axis_index("ep")
    x = x_ref[...].astype(F32)
    xg = (x * g_ref[...]).astype(BF16)
    rows = k_ref.shape[0]
    sums[...] = row_sums(x * x)
    at = 0
    for w_ref in (wq_ref, wk_ref, wv_ref):
        cols = w_ref.shape[1]
        val = jnp.dot(xg, w_ref[...], preferred_element_type=F32).astype(BF16)
        for i in range(n):
            part[i, :, at : at + cols] = val[i * rows : (i + 1) * rows]
        at += cols
    greet((("ep", n),))
    copies = []
    for k in range(1, n):
        peer = lax.rem(me + k, n)
        copies.append(send("ep", n, k, part.at[peer], got.at[k - 1], p_send, p_recv))
        copies.append(send("ep", n, k, sums, got_sums.at[k - 1], s_send, s_recv))
    total = part[me].astype(F32)
    squares = sums[...]
    for k in range(1, n):
        copies[2 * k - 2].wait_recv()
        total = total + got[k - 1].astype(F32)
        copies[2 * k - 1].wait_recv()
        squares = squares + got_sums[k - 1]
    mean = own_column(squares, me * rows, rows) / width
    total = total * lax.rsqrt(mean + EPSILON)
    hd = q_ref.shape[2]
    q_width = wq_ref.shape[1]
    k_width = wk_ref.shape[1]
    for h in range(q_ref.shape[0]):
        q_ref[h] = total[:, h * hd : (h + 1) * hd].astype(BF16).astype(F32)
    k_ref[...] = total[:, q_width : q_width + k_width].astype(BF16)
    v_ref[...] = total[:, q_width + k_width :].astype(BF16)
    for copy in copies:
        copy.wait_send()


def attend_kernel(kv, per, len_ref, off_ref, q_ref, gain_ref, key_ref, val_ref, out_ref):
    step = pl.program_id(0)
    heads = q_ref.shape[0]
    hd = q_ref.shape[2]
    cols = key_ref.shape[1]
    group = heads // kv
    rows = per * heads
    lanes = 128
    blocks = cols // lanes
    q = jnp.concatenate(
        [q_ref[h, pl.ds(step * per + s, 1), :] for s in range(per) for h in range(heads)], axis=0
    ).astype(BF16)
    row = lax.broadcasted_iota(jnp.int32, (rows, lanes), 0)
    lane = lax.broadcasted_iota(jnp.int32, (rows, lanes), 1)
    offset = jnp.zeros((rows, lanes), F32)
    length = jnp.zeros((rows, lanes), jnp.int32)
    for s in range(per):
        length = jnp.where(row // heads == s, len_ref[step * per + s], length)
    for h in range(heads):
        offset = jnp.where(row % heads == h, off_ref[h], offset)
    mine = (row % heads) // group
    scores = jnp.zeros((rows, cols), F32)
    row_all = lax.broadcasted_iota(jnp.int32, (rows, cols), 0)
    for s in range(per):
        one = lax.dot_general(q, key_ref[s], NT, preferred_element_type=F32)
        scores = one if s == 0 else jnp.where(row_all // heads == s, one, scores)
    sigs, valids, fails = [], [], []
    for b in range(blocks):
        sc = scores[:, b * lanes : (b + 1) * lanes] * hd ** (-0.5) + offset
        col = lane + b * lanes
        valid = (col // kv < length) & (col % kv == mine)
        ls = jnp.minimum(sc, 0.0) - jnp.log(1.0 + jnp.exp(-jnp.abs(sc)))
        sigs.append(ls)
        valids.append(valid)
        fails.append(jnp.where(valid, ls - sc, 0.0))
    failed = jnp.concatenate(fails, axis=0)
    high = failed.astype(BF16)
    low = (failed - high.astype(F32)).astype(BF16)
    r = lax.broadcasted_iota(jnp.int32, (lanes, 2 * lanes), 0)
    c = lax.broadcasted_iota(jnp.int32, (lanes, 2 * lanes), 1)
    tri = jnp.where((r > c) | (c >= lanes), 1.0, 0.0).astype(BF16)
    sums = jnp.dot(high, tri, preferred_element_type=F32) + jnp.dot(
        low, tri, preferred_element_type=F32
    )
    acc = jnp.zeros((rows, lanes), F32)
    weights = [None] * blocks
    for b in reversed(range(blocks)):
        later = sums[b * rows : (b + 1) * rows, :lanes] + acc
        acc = acc + sums[b * rows : (b + 1) * rows, lanes:]
        weights[b] = jnp.where(valids[b], jnp.exp(sigs[b] + later), 0.0)
    weights = jnp.concatenate(weights, axis=1).astype(BF16)
    row_out = lax.broadcasted_iota(jnp.int32, (rows, hd), 0)
    att = None
    for s in range(per):
        one = jnp.dot(weights, val_ref[s], preferred_element_type=F32)
        att = one if s == 0 else jnp.where(row_out // heads == s, one, att)
    gains = jnp.concatenate([gain_ref[...]] * per, axis=0)
    att = att * lax.rsqrt(jnp.mean(att * att, axis=1, keepdims=True) + EPSILON) * gains
    for s in range(per):
        for h in range(heads):
            out_ref[h, pl.ds(step * per + s, 1), :] = att[s * heads + h : s * heads + h + 1]


def rest_kernel(
    n, nt, width, cap,
    head_ref, x_ref, fg_ref, mix_ref, slot_row_ref, share_row_ref, slot_col_ref,
    wo_hbm, dg_hbm, du_hbm, dd_hbm, eg_hbm, eu_hbm, ed_hbm,
    out_ref,
    wo, dg, du, dd, eg, eu, ed, w_sem,
    heads_all, part, parts, disp, disp_in, sums, sums_in, gu, gu_in, hid_all, ret, ret_in,
    fin, fins,
    h_send, h_recv, a_send, a_recv, d_send, d_recv, s_send, s_recv, g_send, g_recv,
    i_send, i_recv, r_send, r_recv, f_send, f_recv,
):
    me = lax.axis_index("ep")
    loads = []
    for i, (src, dst) in enumerate(
        ((wo_hbm, wo), (dg_hbm, dg), (du_hbm, du), (eg_hbm.at[0], eg), (eu_hbm.at[0], eu),
         (ed_hbm.at[0], ed), (dd_hbm, dd))
    ):
        load = pltpu.make_async_copy(src, dst, w_sem.at[i])
        load.start()
        loads.append(load)
    total_rows, block = x_ref.shape
    rows = total_rows // n
    heads_all[me] = jnp.concatenate(
        [head_ref[h] for h in range(head_ref.shape[0])], axis=1
    ).astype(BF16)
    greet((("ep", n), ("tp", nt)))
    sent = []
    copies = [
        send("ep", n, k, heads_all.at[me], heads_all.at[me], h_send, h_recv) for k in range(1, n)
    ]
    sent += copies
    slot_rows = lax.broadcasted_iota(jnp.int32, (cap, total_rows), 0)
    loads[0].wait()
    for copy in copies:
        copy.wait_recv()
    all_heads = heads_all[...].reshape(total_rows, heads_all.shape[2])
    part[...] = jnp.dot(all_heads, wo[...], preferred_element_type=F32).astype(BF16)
    copies = [send("tp", nt, k, part, parts.at[k - 1], a_send, a_recv) for k in range(1, nt)]
    sent += copies
    attn = part[...].astype(F32)
    for k in range(1, nt):
        copies[k - 1].wait_recv()
        attn = attn + parts[k - 1].astype(F32)
    residual = x_ref[...].astype(F32) + attn.astype(BF16).astype(F32)
    u = (residual * fg_ref[...]).astype(BF16)
    sums[...] = row_sums(residual * residual)
    slots = [slot_row_ref[k : k + 1, :] for k in range(slot_row_ref.shape[0])]

    def picks(expert):
        place = slot_rows + expert * cap
        return [slot == place for slot in slots]

    d_copies, s_copies = [], []
    for k in range(1, n):
        peer = lax.rem(me + k, n)
        hit = functools.reduce(jnp.logical_or, picks(peer))
        disp[k] = jnp.dot(
            jnp.where(hit, 1.0, 0.0).astype(BF16), u, preferred_element_type=F32
        ).astype(BF16)
        d_copies.append(send("ep", n, k, disp.at[k], disp_in.at[k - 1], d_send, d_recv))
        s_copies.append(send("ep", n, k, sums, sums_in.at[k - 1], s_send, s_recv))
    sent += d_copies + s_copies
    mine = picks(me)
    hit = functools.reduce(jnp.logical_or, mine)
    own_in = jnp.dot(
        jnp.where(hit, 1.0, 0.0).astype(BF16), u, preferred_element_type=F32
    ).astype(BF16)
    hidden = dg.shape[1]
    loads[1].wait()
    val = jnp.dot(u, dg[...], preferred_element_type=F32).astype(BF16)
    for i in range(n):
        gu[i, :, :hidden] = val[i * rows : (i + 1) * rows]
    loads[2].wait()
    val = jnp.dot(u, du[...], preferred_element_type=F32).astype(BF16)
    for i in range(n):
        gu[i, :, hidden:] = val[i * rows : (i + 1) * rows]
    g_copies = [
        send("ep", n, k, gu.at[lax.rem(me + k, n)], gu_in.at[k - 1], g_send, g_recv)
        for k in range(1, n)
    ]
    sent += g_copies
    loads[3].wait()
    loads[4].wait()
    first = pl.ds(pl.multiple_of(me * block, block), block)
    gate = jnp.dot(own_in, eg[first, :], preferred_element_type=F32)
    up = jnp.dot(own_in, eu[first, :], preferred_element_type=F32)
    squares = sums[...]
    for k in range(1, n):
        s_copies[k - 1].wait_recv()
        squares = squares + sums_in[k - 1]
        d_copies[k - 1].wait_recv()
        owner = lax.rem(me - k + n, n)
        span = pl.ds(pl.multiple_of(owner * block, block), block)
        gate = gate + jnp.dot(disp_in[k - 1], eg[span, :], preferred_element_type=F32)
        up = up + jnp.dot(disp_in[k - 1], eu[span, :], preferred_element_type=F32)
    scale_row = lax.rsqrt(squares[0:1, :] / width + EPSILON)
    scale = jnp.sum(jnp.where(hit, scale_row, 0.0), axis=1, keepdims=True)
    share = jnp.zeros((cap, 1), F32)
    for k in range(len(mine)):
        share = share + jnp.sum(
            jnp.where(mine[k], share_row_ref[k : k + 1, :], 0.0), axis=1, keepdims=True
        )
    gate = gate * scale
    up = up * scale
    act = (gate / (1.0 + jnp.exp(-gate)) * up).astype(BF16)
    loads[5].wait()
    for i in range(n):
        ret[i] = (
            jnp.dot(act, ed[:, i * block : (i + 1) * block], preferred_element_type=F32) * share
        ).astype(BF16)
    r_copies = [
        send("ep", n, k, ret.at[lax.rem(me + k, n)], ret_in.at[k - 1], r_send, r_recv)
        for k in range(1, n)
    ]
    sent += r_copies
    gate_up = gu[me].astype(F32)
    for k in range(1, n):
        g_copies[k - 1].wait_recv()
        gate_up = gate_up + gu_in[k - 1].astype(F32)
    gate_up = gate_up * own_column(
        jnp.broadcast_to(scale_row, (8, total_rows)), me * rows, rows
    )
    dense_gate = gate_up[:, :hidden]
    hid_all[me] = (dense_gate / (1.0 + jnp.exp(-dense_gate)) * gate_up[:, hidden:]).astype(BF16)
    i_copies = [
        send("ep", n, k, hid_all.at[me], hid_all.at[me], i_send, i_recv) for k in range(1, n)
    ]
    sent += i_copies
    slot_cols = lax.broadcasted_iota(jnp.int32, (total_rows, cap), 1)
    columns = [slot_col_ref[:, k : k + 1] for k in range(slot_col_ref.shape[1])]

    def combine(expert, rows_in):
        place = slot_cols + expert * cap
        hits = functools.reduce(jnp.logical_or, [column == place for column in columns])
        return jnp.dot(
            jnp.where(hits, 1.0, 0.0).astype(BF16), rows_in, preferred_element_type=F32
        )

    moe = combine(me, ret[me])
    for k in range(1, n):
        r_copies[k - 1].wait_recv()
        moe = moe + combine(lax.rem(me - k + n, n), ret_in[k - 1])
    loads[6].wait()
    for copy in i_copies:
        copy.wait_recv()
    dense = jnp.dot(
        hid_all[...].reshape(total_rows, hidden), dd[...], preferred_element_type=F32
    )
    both = moe + mix_ref[...] * dense
    fin[...] = both.astype(BF16)
    f_copies = [send("tp", nt, k, fin, fins.at[k - 1], f_send, f_recv) for k in range(1, nt)]
    sent += f_copies
    total = residual + fin[...].astype(F32)
    for k in range(1, nt):
        f_copies[k - 1].wait_recv()
        total = total + fins[k - 1].astype(F32)
    out_ref[...] = total.astype(BF16)
    for copy in sent:
        copy.wait_send()


def per_device(
    n, nt, stream, norm_gain, w_query, w_key, w_value, break_offset, cache_keys, cache_values,
    lengths, w_output, head_gain, ffn_gain, route_experts, route_weights, expert_gate,
    expert_up, expert_down, dense_gate, dense_up, dense_down, mix_gain,
):
    total_rows, block = stream.shape
    width = block * n
    rows = lengths.shape[0]
    kv = cache_keys.shape[2]
    hd = cache_keys.shape[3]
    heads = break_offset.shape[0]
    cache_len = cache_keys.shape[1]
    top = route_experts.shape[1]
    hidden = dense_gate.shape[1]
    expert_hidden = expert_gate.shape[2]
    experts = expert_gate.shape[0] * n
    cap = 2 * rows * top // expert_gate.shape[0]
    assert experts == n
    vmem = pl.BlockSpec(memory_space=pltpu.VMEM)
    hbm = pl.BlockSpec(memory_space=pl.ANY)
    dma = pltpu.SemaphoreType.DMA
    limit = 60 * 1024 * 1024

    wide = w_query.shape[1] + w_key.shape[1] + w_value.shape[1]
    queries, key_rows, value_rows = pl.pallas_call(
        functools.partial(project_kernel, n, width),
        out_shape=(
            jax.ShapeDtypeStruct((heads, rows, hd), F32),
            jax.ShapeDtypeStruct((rows, w_key.shape[1]), BF16),
            jax.ShapeDtypeStruct((rows, w_value.shape[1]), BF16),
        ),
        in_specs=[vmem] * 5,
        out_specs=(vmem, vmem, vmem),
        scratch_shapes=[
            pltpu.VMEM((n, rows, wide), BF16),
            pltpu.VMEM((8, total_rows), F32),
            pltpu.VMEM((n - 1, rows, wide), BF16),
            pltpu.VMEM((n - 1, 8, total_rows), F32),
            dma((n - 1,)), dma((n - 1,)), dma((n - 1,)), dma((n - 1,)),
        ],
        compiler_params=pltpu.CompilerParams(collective_id=0, has_side_effects=True),
        name="project",
    )(stream, norm_gain.reshape(1, block), w_query, w_key, w_value)

    per = 2
    flat = kv * cache_len
    smem = pl.BlockSpec(memory_space=pltpu.SMEM)
    head_out = pl.pallas_call(
        functools.partial(attend_kernel, kv, per),
        grid=(rows // per,),
        out_shape=jax.ShapeDtypeStruct((heads, rows, hd), F32),
        in_specs=[
            smem,
            smem,
            pl.BlockSpec((heads, rows, hd), lambda i: (0, 0, 0)),
            pl.BlockSpec((heads, hd), lambda i: (0, 0)),
            pl.BlockSpec((per, flat, hd), lambda i: (i, 0, 0)),
            pl.BlockSpec((per, flat, hd), lambda i: (i, 0, 0)),
        ],
        out_specs=pl.BlockSpec((heads, rows, hd), lambda i: (0, 0, 0)),
        compiler_params=pltpu.CompilerParams(dimension_semantics=("arbitrary",)),
        name="attend",
    )(
        lengths,
        break_offset,
        queries,
        head_gain.reshape(heads, hd),
        cache_keys.reshape(rows, flat, hd),
        cache_values.reshape(rows, flat, hd),
    )

    chosen = route_experts.reshape(-1)
    pair = jnp.arange(chosen.shape[0], dtype=jnp.int32)
    earlier = (chosen[None, :] == chosen[:, None]) & (pair[None, :] < pair[:, None])
    slot_ids = chosen * cap + jnp.sum(earlier.astype(jnp.int32), axis=1)
    slot_ids = slot_ids.reshape(total_rows, top)
    shares = route_weights / jnp.sum(route_weights, axis=1, keepdims=True)

    dt = w_output.shape[0]
    return_shape = (n, cap, block)
    mixed_out = pl.pallas_call(
        functools.partial(rest_kernel, n, nt, width, cap),
        out_shape=jax.ShapeDtypeStruct((total_rows, block), BF16),
        in_specs=[vmem] * 7 + [hbm] * 7,
        out_specs=vmem,
        scratch_shapes=[
            pltpu.VMEM(w_output.shape, BF16),
            pltpu.VMEM(dense_gate.shape, BF16),
            pltpu.VMEM(dense_up.shape, BF16),
            pltpu.VMEM(dense_down.shape, BF16),
            pltpu.VMEM(expert_gate.shape[1:], BF16),
            pltpu.VMEM(expert_up.shape[1:], BF16),
            pltpu.VMEM(expert_down.shape[1:], BF16),
            dma((7,)),
            pltpu.VMEM((n, rows, dt), BF16),
            pltpu.VMEM((total_rows, block), BF16),
            pltpu.VMEM((nt - 1, total_rows, block), BF16),
            pltpu.VMEM(return_shape, BF16),
            pltpu.VMEM((n - 1, cap, block), BF16),
            pltpu.VMEM((8, total_rows), F32),
            pltpu.VMEM((n - 1, 8, total_rows), F32),
            pltpu.VMEM((n, rows, 2 * hidden), BF16),
            pltpu.VMEM((n - 1, rows, 2 * hidden), BF16),
            pltpu.VMEM((n, rows, hidden), BF16),
            pltpu.VMEM(return_shape, BF16),
            pltpu.VMEM((n - 1, cap, block), BF16),
            pltpu.VMEM((total_rows, block), BF16),
            pltpu.VMEM((nt - 1, total_rows, block), BF16),
            dma((n - 1,)), dma((n - 1,)), dma((nt - 1,)), dma((nt - 1,)),
            dma((n - 1,)), dma((n - 1,)), dma((n - 1,)), dma((n - 1,)),
            dma((n - 1,)), dma((n - 1,)), dma((n - 1,)), dma((n - 1,)),
            dma((n - 1,)), dma((n - 1,)), dma((nt - 1,)), dma((nt - 1,)),
        ],
        compiler_params=pltpu.CompilerParams(
            collective_id=1, has_side_effects=True, vmem_limit_bytes=limit
        ),
        name="rest",
    )(
        head_out, stream, ffn_gain.reshape(1, block), mix_gain.reshape(1, block),
        slot_ids.T, shares.T, slot_ids,
        w_output, dense_gate, dense_up, dense_down, expert_gate, expert_up, expert_down,
    )
    return (mixed_out, key_rows, value_rows)


def solution(mesh):
    in_specs = (
        P(None, "ep"),
        P("ep"),
        P("ep", "tp"),
        P("ep", "tp"),
        P("ep", "tp"),
        P("tp"),
        P("ep", None, "tp", None),
        P("ep", None, "tp", None),
        P("ep"),
        P("tp", "ep"),
        P("tp"),
        P("ep"),
        P(),
        P(),
        P("ep", None, "tp"),
        P("ep", None, "tp"),
        P("ep", "tp", None),
        P("ep", "tp"),
        P("ep", "tp"),
        P("tp", "ep"),
        P("ep"),
    )
    out_specs = (P(None, "ep"), P("ep", "tp"), P("ep", "tp"))
    body = functools.partial(per_device, mesh.shape["ep"], mesh.shape["tp"])
    return jax.shard_map(
        body, mesh=mesh, in_specs=in_specs, out_specs=out_specs, check_vma=False
    )
```

time: 458 us -> 99.9 us (0.22)
  waiting for transfers between devices: 155 us -> 0 us
  blocking collectives: 120 us -> 0 us
  other arithmetic: 110 us -> 2.82 us
  Pallas kernels: 0 us -> 90.7 us
  matrix products: 25.7 us -> 0 us
  local copies, waits for them, and re-layouts: 25.2 us -> 3.93 us
  between operations: 14.2 us -> 0.69 us
  starting transfers between devices: 6.96 us -> 0 us
    reduce_scatter x3 -> x0, waiting for transfers between devices: 103 us -> none  [the longest x2 103 us: to_heads(): lax.psum_scatter(jnp.dot(normed, weights, preferred_element_type=jnp.floa...]
    pallas_call x0 -> x3, Pallas kernels: none -> 90.7 us  [the longest x1 65.1 us: per_device(): pl.pallas_call(functools.partial(rest_kernel, n, nt, width, cap), out_sha...]
    another operation x5 -> x0, other arithmetic: 80 us -> none
    all_gather x4 -> x0, blocking collectives: 75.3 us -> none  [the longest x2 61.4 us: from_heads(): lax.all_gather(values, 'ep', axis=0, tiled=True)]
    psum x2 -> x0, blocking collectives: 44.5 us -> none  [rms_scale(): squares = lax.psum(jnp.sum(values * values, axis=1), 'ep')]
    psum x2 -> x0, waiting for transfers between devices: 42.3 us -> none  [from_heads(): return lax.psum(partial_value.astype(jnp.bfloat16), 'tp')]
    dot_general x8 -> x0, matrix products: 25.7 us -> none  [the longest x1 5.89 us: per_device(): jnp.einsum('skgl,slkd->skgd', weights, cache_values, preferred_element_ty...]
    unnamed x1 -> x0, other arithmetic: 23.4 us -> none
  transfers between devices with their start and end apart: 7 -> 0, of which waited for: 6 -> 0; matrix products, arithmetic and copies ran while one was open for 6% -> 0% of each run, Pallas kernels for 0% -> 0%
where the time goes in v1:
time: 99.9 us; the launch traced here: 98.1 us
  Pallas kernels  90.7 us (91%)
  local copies, waits for them, and re-layouts  3.93 us (4%)
  other arithmetic  2.82 us (3%)
    pallas_call x1, Pallas kernels, per_device(): pl.pallas_call(functools.partial(rest_kernel, n, nt, width, cap), out_sha...  65.1 us
    pallas_call x1, Pallas kernels, per_device(): pl.pallas_call(functools.partial(project_kernel, n, width), out_shape=(ja...  13.7 us
    pallas_call x1, Pallas kernels, per_device(): pl.pallas_call(functools.partial(attend_kernel, kv, per), grid=(rows // p...  11.9 us
    unnamed x12, local copies, waits for them, and re-layouts  2.9 us

profile of v1, /device:TPU:0, one launch (start us, length us, event | category | flops | bytes accessed | tf_op | source)
XLA Modules:
  0.0 98.1 jit_solution(3461110303795096727)
XLA Ops:
  0.6 0.7 reduce_sum.22
  1.3 1.2 %divide_bitcast_fusion.share_row_ref = f32[2,128]{1,0:T(2,128)} fusion(f32[128,2]{0,1:T(2,128)} %param.34, f32[128]{0:T(128)S(1)} %reduce_sum.22), kind=kLoop, calls=%fused_computation.3 | loop fusion | flops 256 | bytes 2560 | tf_op jit(solution)/shard_map/transpose | solution.py:445
  2.6 0.7 broadcast_multiply_fusion
  3.3 13.7 %project.1 = (f32[4,16,128]{2,1,0:T(8,128)}, bf16[16,256]{1,0:T(8,128)(2,1)}, bf16[16,256]{1,0:T(8,128)(2,1)}) custom-call(bf16[128,512]{1,0:T(8,128)(2,1)} %x_ref.3, f32[1,512]{1,0:T(1,128)} %bitcast.12, bf16[512,512]{1,0:T(8,128)(2,1)} %wq_ref.1, bf16[512,256]{1,0:T(8,128)(2,1)} %wk_ref.1, bf16[512,256]{1,0:T(8,128)(2,1)} %wv_ref.1), custom_call_target="tpu_custom_call" | custom-call | tf_op jit(solution)/shard_map/project/pallas_call | solution.py:350
  17.0 0.0 copy-start.3
  17.0 11.9 %attend.1.head_ref = f32[4,16,128]{2,1,0:T(8,128)} custom-call(s32[16]{0:T(128)} %len_ref.1, f32[4]{0:T(128)} %off_ref.1, f32[4,16,128]{2,1,0:T(8,128)} %get-tuple-element.6.q_ref, f32[4,128]{1,0:T(4,128)} %bitcast.13, bf16[16,2048,128]{2,1,0:T(8,128)(2,1)} %bitcast.9, bf16[16,2048,128]{2,1,0:T(8,128)(2,1)} %bitcast.10), custom_call_target="tpu_custom_call" | custom-call | tf_op jit(solution)/shard_map/attend/pallas_call | solution.py:373
  28.9 0.1 copy.36
  29.0 0.0 copy-done.3
  29.0 0.1 copy.35
  29.1 0.1 eq.15
  29.3 0.2 convert_reduce_fusion
  29.5 0.1 reduce_sum.21
  29.6 0.0 copy-start
  29.7 0.6 copy.37.slot_row_ref
  30.3 0.0 copy-done
  30.3 0.0 copy-start.2
  30.3 0.0 copy-start.1
  30.3 65.1 %rest.1 = bf16[128,512]{1,0:T(8,128)(2,1)} custom-call(f32[4,16,128]{2,1,0:T(8,128)} %attend.1.head_ref, bf16[128,512]{1,0:T(8,128)(2,1)} %x_ref.3, f32[1,512]{1,0:T(1,128)} %bitcast.14, f32[1,512]{1,0:T(1,128)} %bitcast.15, s32[2,128]{1,0:T(2,128)} %copy.37.slot_row_ref, f32[2,128]{1,0:T(2,128)} %divide_bitcast_fusion.share_row_ref, s32[128,2]{1,0:T(8,128)} %copy-done, ...), custom_call_target="tpu_custom_call" | custom-call | tf_op jit(solution)/shard_map/rest/pallas_call | solution.py:406
  95.4 1.6 %copy.41 = bf16[128,512]{1,0:T(8,128)(2,1)} copy(bf16[128,512]{1,0:T(8,128)(2,1)} %rest.1) | data formatting | bytes 262144
  96.9 0.0 copy-done.2
  96.9 0.6 copy.42
  97.5 0.0 copy-done.1
  97.5 0.6 copy.43
  (1 shorter events, 0.0 us)
Async XLA Ops:
  17.0 12.0 %copy-start.3 = (s32[128,2]{0,1:T(2,128)S(1)}, s32[128,2]{0,1:T(2,128)}, u32[]{:S(2)}) copy-start(s32[128,2]{0,1:T(2,128)} %param.33) | copy-start | bytes 3076
  29.6 0.7 copy-start
  30.3 66.7 %copy-start.2 = (bf16[16,256]{1,0:T(8,128)(2,1)S(1)}, bf16[16,256]{1,0:T(8,128)(2,1)}, u32[]{:S(2)}) copy-start(bf16[16,256]{1,0:T(8,128)(2,1)} %get-tuple-element.13) | copy-start | bytes 24580
  30.3 67.3 %copy-start.1 = (bf16[16,256]{1,0:T(8,128)(2,1)S(1)}, bf16[16,256]{1,0:T(8,128)(2,1)}, u32[]{:S(2)}) copy-start(bf16[16,256]{1,0:T(8,128)(2,1)} %get-tuple-element.14) | copy-start | bytes 24580

commit v2 on v1

--- a/solution.py
+++ b/solution.py
@@ -55,6 +55,44 @@
     )
     copy.start()
     return copy
+
+
+def send_to(peer, src, dst, sems, i):
+    copy = pltpu.make_async_remote_copy(
+        src_ref=src,
+        dst_ref=dst,
+        send_sem=sems[0].at[i],
+        recv_sem=sems[1].at[i],
+        device_id={"tp": peer},
+        device_id_type=MESH,
+    )
+    copy.start()
+    return copy
+
+
+def tp_sum(nt, part, arrived, pair, crossed, full, sems, extra):
+    me = lax.axis_index("tp")
+    core = lax.rem(me, 2)
+    partner = me + 1 - 2 * core
+    half = pair.shape[0]
+    mine = pl.ds(pl.multiple_of(core * half, half), half)
+    other = pl.ds(pl.multiple_of((1 - core) * half, half), half)
+    copies = [send_to(partner, part.at[other], arrived, sems, 0)]
+    copies[0].wait_recv()
+    pair[...] = (part[mine].astype(F32) + arrived[...].astype(F32)).astype(BF16)
+    for j in range(1, nt // 2):
+        copies.append(send_to(lax.rem(me + 2 * j, nt), pair, crossed.at[j - 1], sems, j))
+    total = pair[...].astype(F32)
+    for j in range(1, nt // 2):
+        copies[j].wait_recv()
+        total = total + crossed[j - 1].astype(F32)
+    if extra is not None:
+        total = total + extra[mine]
+    full[mine] = total.astype(BF16)
+    copies.append(send_to(partner, full.at[mine], full.at[mine], sems, nt // 2))
+    copies[-1].wait_recv()
+    for copy in copies:
+        copy.wait_send()
 
 
 def project_kernel(
@@ -99,8 +137,11 @@
         copy.wait_send()
 
 
-def attend_kernel(kv, per, len_ref, off_ref, q_ref, gain_ref, key_ref, val_ref, out_ref):
+def attend_kernel(kv, per, len_ref, off_ref, q_ref, gain_ref, new_k_ref, new_v_ref, key_ref, val_ref,
+                  out_ref, k_out_ref, v_out_ref):
     step = pl.program_id(0)
+    k_out_ref[...] = new_k_ref[...]
+    v_out_ref[...] = new_v_ref[...]
     heads = q_ref.shape[0]
     hd = q_ref.shape[2]
     cols = key_ref.shape[1]
@@ -164,14 +205,15 @@
 
 def rest_kernel(
     n, nt, width, cap,
-    head_ref, x_ref, fg_ref, mix_ref, slot_row_ref, share_row_ref, slot_col_ref,
+    head_ref, x_ref, fg_ref, mix_ref, route_ref, route_w_ref,
     wo_hbm, dg_hbm, du_hbm, dd_hbm, eg_hbm, eu_hbm, ed_hbm,
     out_ref,
     wo, dg, du, dd, eg, eu, ed, w_sem,
-    heads_all, part, parts, disp, disp_in, sums, sums_in, gu, gu_in, hid_all, ret, ret_in,
-    fin, fins,
-    h_send, h_recv, a_send, a_recv, d_send, d_recv, s_send, s_recv, g_send, g_recv,
-    i_send, i_recv, r_send, r_recv, f_send, f_recv,
+    heads_all, part, disp, disp_in, sums, sums_in, gu, gu_in, hid_all, act_s, share_s,
+    ret_x, ret_p, ret_m, ret, ret_in, res,
+    a_in, a_pair, a_cross, a_full, f_in, f_pair, f_cross, f_full,
+    h_send, h_recv, d_send, d_recv, w_send, w_recv, s_send, s_recv, g_send, g_recv,
+    i_send, i_recv, r_send, r_recv, a_send, a_recv, f_send, f_recv, x_send, x_recv,
 ):
     me = lax.axis_index("ep")
     loads = []
@@ -193,38 +235,66 @@
         send("ep", n, k, heads_all.at[me], heads_all.at[me], h_send, h_recv) for k in range(1, n)
     ]
     sent += copies
+    me_t = lax.axis_index("tp")
+    core = lax.rem(me_t, 2)
+    partner = me_t + 1 - 2 * core
+    half = cap // 2
+    near = pl.ds(pl.multiple_of(core * half, half), half)
+    far = pl.ds(pl.multiple_of((1 - core) * half, half), half)
+    top = route_ref.shape[0]
+    expert_ids = lax.broadcasted_iota(jnp.int32, (n, total_rows), 0)
+    named = [
+        jnp.where(route_ref[k : k + 1, :] == expert_ids, 1.0, 0.0).astype(F32)
+        for k in range(top)
+    ]
+    token_r = lax.broadcasted_iota(jnp.int32, (total_rows, total_rows), 0)
+    token_c = lax.broadcasted_iota(jnp.int32, (total_rows, total_rows), 1)
+    before = jnp.dot(
+        sum(named).astype(BF16),
+        jnp.where(token_r < token_c, 1.0, 0.0).astype(BF16),
+        preferred_element_type=F32,
+    )
+    slots = [
+        jnp.sum(named[k] * before, axis=0, keepdims=True)
+        + route_ref[k : k + 1, :].astype(F32) * cap
+        for k in range(top)
+    ]
+    columns = [
+        jnp.sum(jnp.where(token_r == token_c, slot, 0.0), axis=1, keepdims=True)
+        for slot in slots
+    ]
+    share_sum = route_w_ref[0:1, :]
+    for k in range(1, top):
+        share_sum = share_sum + route_w_ref[k : k + 1, :]
+    share_rows = [route_w_ref[k : k + 1, :] / share_sum for k in range(top)]
     slot_rows = lax.broadcasted_iota(jnp.int32, (cap, total_rows), 0)
+    half_rows = lax.broadcasted_iota(jnp.int32, (half, total_rows), 0) + core * half
     loads[0].wait()
     for copy in copies:
         copy.wait_recv()
     all_heads = heads_all[...].reshape(total_rows, heads_all.shape[2])
     part[...] = jnp.dot(all_heads, wo[...], preferred_element_type=F32).astype(BF16)
-    copies = [send("tp", nt, k, part, parts.at[k - 1], a_send, a_recv) for k in range(1, nt)]
-    sent += copies
-    attn = part[...].astype(F32)
-    for k in range(1, nt):
-        copies[k - 1].wait_recv()
-        attn = attn + parts[k - 1].astype(F32)
-    residual = x_ref[...].astype(F32) + attn.astype(BF16).astype(F32)
+    tp_sum(nt, part, a_in, a_pair, a_cross, a_full, (a_send, a_recv), None)
+    residual = x_ref[...].astype(F32) + a_full[...].astype(F32)
     u = (residual * fg_ref[...]).astype(BF16)
     sums[...] = row_sums(residual * residual)
-    slots = [slot_row_ref[k : k + 1, :] for k in range(slot_row_ref.shape[0])]
-
-    def picks(expert):
-        place = slot_rows + expert * cap
+    res[...] = residual
+
+    def picks(expert, places):
+        place = (places + expert * cap).astype(F32)
         return [slot == place for slot in slots]
 
     d_copies, s_copies = [], []
     for k in range(1, n):
         peer = lax.rem(me + k, n)
-        hit = functools.reduce(jnp.logical_or, picks(peer))
+        hit = functools.reduce(jnp.logical_or, picks(peer, half_rows))
         disp[k] = jnp.dot(
             jnp.where(hit, 1.0, 0.0).astype(BF16), u, preferred_element_type=F32
         ).astype(BF16)
-        d_copies.append(send("ep", n, k, disp.at[k], disp_in.at[k - 1], d_send, d_recv))
+        d_copies.append(send("ep", n, k, disp.at[k], disp_in.at[k - 1, near], d_send, d_recv))
         s_copies.append(send("ep", n, k, sums, sums_in.at[k - 1], s_send, s_recv))
     sent += d_copies + s_copies
-    mine = picks(me)
+    mine = picks(me, slot_rows)
     hit = functools.reduce(jnp.logical_or, mine)
     own_in = jnp.dot(
         jnp.where(hit, 1.0, 0.0).astype(BF16), u, preferred_element_type=F32
@@ -249,29 +319,57 @@
     gate = jnp.dot(own_in, eg[first, :], preferred_element_type=F32)
     up = jnp.dot(own_in, eu[first, :], preferred_element_type=F32)
     squares = sums[...]
-    for k in range(1, n):
-        s_copies[k - 1].wait_recv()
-        squares = squares + sums_in[k - 1]
-        d_copies[k - 1].wait_recv()
-        owner = lax.rem(me - k + n, n)
-        span = pl.ds(pl.multiple_of(owner * block, block), block)
-        gate = gate + jnp.dot(disp_in[k - 1], eg[span, :], preferred_element_type=F32)
-        up = up + jnp.dot(disp_in[k - 1], eu[span, :], preferred_element_type=F32)
+    forwards = []
+    for k in range(1, n + 1):
+        if k < n:
+            d_copies[k - 1].wait_recv()
+            forwards.append(
+                send_to(
+                    partner, disp_in.at[k - 1, near], disp_in.at[k - 1, near],
+                    (w_send, w_recv), k - 1,
+                )
+            )
+        if k > 1:
+            p = k - 1
+            s_copies[p - 1].wait_recv()
+            squares = squares + sums_in[p - 1]
+            forwards[p - 1].wait_recv()
+            owner = lax.rem(me - p + n, n)
+            span = pl.ds(pl.multiple_of(owner * block, block), block)
+            gate = gate + jnp.dot(disp_in[p - 1], eg[span, :], preferred_element_type=F32)
+            up = up + jnp.dot(disp_in[p - 1], eu[span, :], preferred_element_type=F32)
+    sent += forwards
     scale_row = lax.rsqrt(squares[0:1, :] / width + EPSILON)
     scale = jnp.sum(jnp.where(hit, scale_row, 0.0), axis=1, keepdims=True)
     share = jnp.zeros((cap, 1), F32)
     for k in range(len(mine)):
         share = share + jnp.sum(
-            jnp.where(mine[k], share_row_ref[k : k + 1, :], 0.0), axis=1, keepdims=True
+            jnp.where(mine[k], share_rows[k], 0.0), axis=1, keepdims=True
         )
     gate = gate * scale
     up = up * scale
-    act = (gate / (1.0 + jnp.exp(-gate)) * up).astype(BF16)
+    act_s[...] = (gate / (1.0 + jnp.exp(-gate)) * up).astype(BF16)
+    share_s[...] = jnp.broadcast_to(share, share_s.shape)
     loads[5].wait()
+    act_far = act_s[far]
+    share_far = share_s[far][:, 0:1]
     for i in range(n):
-        ret[i] = (
-            jnp.dot(act, ed[:, i * block : (i + 1) * block], preferred_element_type=F32) * share
+        ret_x[i] = (
+            jnp.dot(act_far, ed[:, i * block : (i + 1) * block], preferred_element_type=F32)
+            * share_far
         ).astype(BF16)
+    swap = send_to(partner, ret_x, ret_p, (x_send, x_recv), 0)
+    sent.append(swap)
+    act_near = act_s[near]
+    share_near = share_s[near][:, 0:1]
+    for i in range(n):
+        ret_m[i] = (
+            jnp.dot(act_near, ed[:, i * block : (i + 1) * block], preferred_element_type=F32)
+            * share_near
+        )
+    swap.wait_recv()
+    for i in range(n):
+        ret[i] = (ret_m[i] + ret_p[i].astype(F32)).astype(BF16)
     r_copies = [
         send("ep", n, k, ret.at[lax.rem(me + k, n)], ret_in.at[k - 1], r_send, r_recv)
         for k in range(1, n)
@@ -290,11 +388,9 @@
         send("ep", n, k, hid_all.at[me], hid_all.at[me], i_send, i_recv) for k in range(1, n)
     ]
     sent += i_copies
-    slot_cols = lax.broadcasted_iota(jnp.int32, (total_rows, cap), 1)
-    columns = [slot_col_ref[:, k : k + 1] for k in range(slot_col_ref.shape[1])]
-
+    slot_cols = lax.broadcasted_iota(jnp.int32, (total_rows, half), 1) + core * half
     def combine(expert, rows_in):
-        place = slot_cols + expert * cap
+        place = (slot_cols + expert * cap).astype(F32)
         hits = functools.reduce(jnp.logical_or, [column == place for column in columns])
         return jnp.dot(
             jnp.where(hits, 1.0, 0.0).astype(BF16), rows_in, preferred_element_type=F32
@@ -311,14 +407,9 @@
         hid_all[...].reshape(total_rows, hidden), dd[...], preferred_element_type=F32
     )
     both = moe + mix_ref[...] * dense
-    fin[...] = both.astype(BF16)
-    f_copies = [send("tp", nt, k, fin, fins.at[k - 1], f_send, f_recv) for k in range(1, nt)]
-    sent += f_copies
-    total = residual + fin[...].astype(F32)
-    for k in range(1, nt):
-        f_copies[k - 1].wait_recv()
-        total = total + fins[k - 1].astype(F32)
-    out_ref[...] = total.astype(BF16)
+    part[...] = both.astype(BF16)
+    tp_sum(nt, part, f_in, f_pair, f_cross, f_full, (f_send, f_recv), res)
+    out_ref[...] = f_full[...]
     for copy in sent:
         copy.wait_send()
 
@@ -370,19 +461,27 @@
     per = 2
     flat = kv * cache_len
     smem = pl.BlockSpec(memory_space=pltpu.SMEM)
-    head_out = pl.pallas_call(
+    k_block = pl.BlockSpec(key_rows.shape, lambda i: (0, 0))
+    v_block = pl.BlockSpec(value_rows.shape, lambda i: (0, 0))
+    head_out, key_rows, value_rows = pl.pallas_call(
         functools.partial(attend_kernel, kv, per),
         grid=(rows // per,),
-        out_shape=jax.ShapeDtypeStruct((heads, rows, hd), F32),
+        out_shape=(
+            jax.ShapeDtypeStruct((heads, rows, hd), F32),
+            jax.ShapeDtypeStruct(key_rows.shape, BF16),
+            jax.ShapeDtypeStruct(value_rows.shape, BF16),
+        ),
         in_specs=[
             smem,
             smem,
             pl.BlockSpec((heads, rows, hd), lambda i: (0, 0, 0)),
             pl.BlockSpec((heads, hd), lambda i: (0, 0)),
+            k_block,
+            v_block,
             pl.BlockSpec((per, flat, hd), lambda i: (i, 0, 0)),
             pl.BlockSpec((per, flat, hd), lambda i: (i, 0, 0)),
         ],
-        out_specs=pl.BlockSpec((heads, rows, hd), lambda i: (0, 0, 0)),
+        out_specs=(pl.BlockSpec((heads, rows, hd), lambda i: (0, 0, 0)), k_block, v_block),
         compiler_params=pltpu.CompilerParams(dimension_semantics=("arbitrary",)),
         name="attend",
     )(
@@ -390,23 +489,20 @@
         break_offset,
         queries,
         head_gain.reshape(heads, hd),
+        key_rows,
+        value_rows,
         cache_keys.reshape(rows, flat, hd),
         cache_values.reshape(rows, flat, hd),
     )
 
-    chosen = route_experts.reshape(-1)
-    pair = jnp.arange(chosen.shape[0], dtype=jnp.int32)
-    earlier = (chosen[None, :] == chosen[:, None]) & (pair[None, :] < pair[:, None])
-    slot_ids = chosen * cap + jnp.sum(earlier.astype(jnp.int32), axis=1)
-    slot_ids = slot_ids.reshape(total_rows, top)
-    shares = route_weights / jnp.sum(route_weights, axis=1, keepdims=True)
-
     dt = w_output.shape[0]
-    return_shape = (n, cap, block)
+    assert nt % 2 == 0 and cap % 2 == 0
+    half_cap = (n, cap // 2, block)
+    half_rows = (total_rows // 2, block)
     mixed_out = pl.pallas_call(
         functools.partial(rest_kernel, n, nt, width, cap),
         out_shape=jax.ShapeDtypeStruct((total_rows, block), BF16),
-        in_specs=[vmem] * 7 + [hbm] * 7,
+        in_specs=[vmem] * 6 + [hbm] * 7,
         out_specs=vmem,
         scratch_shapes=[
             pltpu.VMEM(w_output.shape, BF16),
@@ -419,22 +515,33 @@
             dma((7,)),
             pltpu.VMEM((n, rows, dt), BF16),
             pltpu.VMEM((total_rows, block), BF16),
-            pltpu.VMEM((nt - 1, total_rows, block), BF16),
-            pltpu.VMEM(return_shape, BF16),
+            pltpu.VMEM(half_cap, BF16),
             pltpu.VMEM((n - 1, cap, block), BF16),
             pltpu.VMEM((8, total_rows), F32),
             pltpu.VMEM((n - 1, 8, total_rows), F32),
             pltpu.VMEM((n, rows, 2 * hidden), BF16),
             pltpu.VMEM((n - 1, rows, 2 * hidden), BF16),
             pltpu.VMEM((n, rows, hidden), BF16),
-            pltpu.VMEM(return_shape, BF16),
-            pltpu.VMEM((n - 1, cap, block), BF16),
+            pltpu.VMEM((cap, expert_hidden), BF16),
+            pltpu.VMEM((cap, 128), F32),
+            pltpu.VMEM(half_cap, BF16),
+            pltpu.VMEM(half_cap, BF16),
+            pltpu.VMEM(half_cap, F32),
+            pltpu.VMEM(half_cap, BF16),
+            pltpu.VMEM((n - 1, cap // 2, block), BF16),
+            pltpu.VMEM((total_rows, block), F32),
+        ]
+        + [
+            pltpu.VMEM(half_rows, BF16),
+            pltpu.VMEM(half_rows, BF16),
+            pltpu.VMEM((nt // 2 - 1,) + half_rows, BF16),
             pltpu.VMEM((total_rows, block), BF16),
-            pltpu.VMEM((nt - 1, total_rows, block), BF16),
-            dma((n - 1,)), dma((n - 1,)), dma((nt - 1,)), dma((nt - 1,)),
-            dma((n - 1,)), dma((n - 1,)), dma((n - 1,)), dma((n - 1,)),
-            dma((n - 1,)), dma((n - 1,)), dma((n - 1,)), dma((n - 1,)),
-            dma((n - 1,)), dma((n - 1,)), dma((nt - 1,)), dma((nt - 1,)),
+        ] * 2
+        + [dma((n - 1,))] * 14
+        + [dma((nt // 2 + 1,))] * 4
+        + [
+            dma((1,)),
+            dma((1,)),
         ],
         compiler_params=pltpu.CompilerParams(
             collective_id=1, has_side_effects=True, vmem_limit_bytes=limit
@@ -442,7 +549,7 @@
         name="rest",
     )(
         head_out, stream, ffn_gain.reshape(1, block), mix_gain.reshape(1, block),
-        slot_ids.T, shares.T, slot_ids,
+        route_experts.T, route_weights.T,
         w_output, dense_gate, dense_up, dense_down, expert_gate, expert_up, expert_down,
     )
     return (mixed_out, key_rows, value_rows)

time: 99.9 us -> 81.4 us (0.81); the launches traced: 98.1 us -> 81.1 us
  Pallas kernels: 90.7 us -> 78.9 us
  other arithmetic: 2.82 us -> 0 us
  local copies, waits for them, and re-layouts: 3.93 us -> 1.57 us
    pallas_call x1, Pallas kernels: 65.1 us -> 53.2 us  [per_device(): pl.pallas_call(functools.partial(rest_kernel, n, nt, width, cap), out_sha...]
    unnamed x12 -> x1, local copies, waits for them, and re-layouts: 2.9 us -> 1.57 us
    transpose x1 -> x0, other arithmetic: 1.25 us -> none  [per_device(): mixed_out = pl.pallas_call(functools.partial(rest_kernel, n, nt, width, c...]
where the time goes in v2:
time: 81.4 us; the launch traced here: 81.1 us
  Pallas kernels  78.9 us (97%)
  local copies, waits for them, and re-layouts  1.57 us (2%)
    pallas_call x1, Pallas kernels, per_device(): pl.pallas_call(functools.partial(rest_kernel, n, nt, width, cap), out_sha...  53.2 us
    pallas_call x1, Pallas kernels, per_device(): pl.pallas_call(functools.partial(project_kernel, n, width), out_shape=(ja...  13.7 us
    pallas_call x1, Pallas kernels, per_device(): pl.pallas_call(functools.partial(attend_kernel, kv, per), grid=(rows // p...  11.9 us

profile of v2, /device:TPU:0, one launch (start us, length us, event | category | flops | bytes accessed | tf_op | source)
XLA Modules:
  0.0 81.1 jit_solution(8992459079575657541)
XLA Ops:
  0.6 13.7 %project.1 = (f32[4,16,128]{2,1,0:T(8,128)}, bf16[16,256]{1,0:T(8,128)(2,1)}, bf16[16,256]{1,0:T(8,128)(2,1)}) custom-call(bf16[128,512]{1,0:T(8,128)(2,1)} %x_ref.3, f32[1,512]{1,0:T(1,128)} %bitcast.10, bf16[512,512]{1,0:T(8,128)(2,1)} %wq_ref.1, bf16[512,256]{1,0:T(8,128)(2,1)} %wk_ref.1, bf16[512,256]{1,0:T(8,128)(2,1)} %wv_ref.1), custom_call_target="tpu_custom_call" | custom-call | tf_op jit(solution)/shard_map/project/pallas_call | solution.py:441
  14.4 11.9 %attend.1 = (f32[4,16,128]{2,1,0:T(8,128)}, bf16[16,256]{1,0:T(8,128)(2,1)}, bf16[16,256]{1,0:T(8,128)(2,1)}) custom-call(s32[16]{0:T(128)} %len_ref.1, f32[4]{0:T(128)} %off_ref.1, f32[4,16,128]{2,1,0:T(8,128)} %get-tuple-element.9.q_ref, f32[4,128]{1,0:T(4,128)} %bitcast.13, bf16[16,256]{1,0:T(8,128)(2,1)} %get-tuple-element.10.new_k_ref, ...), custom_call_target="tpu_custom_call" | custom-call | tf_op jit(solution)/shard_map/attend/pallas_call | solution.py:466
  26.3 53.2 %rest.1 = bf16[128,512]{1,0:T(8,128)(2,1)} custom-call(f32[4,16,128]{2,1,0:T(8,128)} %get-tuple-element.12.head_ref, bf16[128,512]{1,0:T(8,128)(2,1)} %x_ref.3, f32[1,512]{1,0:T(1,128)} %bitcast.11, f32[1,512]{1,0:T(1,128)} %bitcast.12, s32[2,128]{1,0:T(2,128)} %bitcast.14, f32[2,128]{1,0:T(2,128)} %bitcast.15, bf16[512,512]{1,0:T(8,128)(2,1)} %wo_hbm.1, ...), custom_call_target="tpu_custom_call" | custom-call | tf_op jit(solution)/shard_map/rest/pallas_call | solution.py:502
  79.5 1.6 %copy.25 = bf16[128,512]{1,0:T(8,128)(2,1)} copy(bf16[128,512]{1,0:T(8,128)(2,1)} %rest.1) | data formatting | bytes 262144
